TPU v7x, 32 devices: a whole 2x2x4 slice. The times are simulated.
32 devices in a mesh: sp: 16 (over z, y, core), tp: 2 (over x).
Axes of the slice: x: 2, y: 2, z: 4, core: 2. Of those that a mesh axis runs over, the one named last changes fastest.
Arguments:
- query_rows: bfloat16 [8192, 1024], P(('sp', 'tp')), may hold values from -6 to 6
- key_rows: bfloat16 [8192, 1024], P(('sp', 'tp')), may hold values from -6 to 6
- value_rows: bfloat16 [8192, 1024], P(('sp', 'tp')), may hold values from -6 to 6
- out_grad: bfloat16 [8192, 1024], P(('sp', 'tp')), may hold values from -40 to 40
- log_totals: float32 [8192, 8], P(('sp', 'tp')), may hold values from 6 to 7.5
- out_dot: float32 [8192, 8], P(('sp', 'tp')), may hold values from -6 to 6
- bias_table: float32 [8, 320], replicated, may hold values from -4 to 4
Outputs:
- grad_query: bfloat16 [8192, 1024], P(('sp', 'tp'))
- grad_key: bfloat16 [8192, 1024], P(('sp', 'tp'))
- grad_value: bfloat16 [8192, 1024], P(('sp', 'tp'))
- grad_table: float32 [8, 320], replicated
All inputs are finite; a program needn't handle non-finite values.
Results may differ from a plain program's by a relative error of at most 0.005.
Values may be sent and summed in bfloat16 or wider, within the bound.
No kernel may reach another device: no remote copies, remote signals or barrier semaphores. Data moves between devices by JAX's collectives and lax.ppermute only.
A program may use at most 128 MiB of HBM per device.

v0:
```python
import jax
import jax.numpy as jnp
from jax import lax
from jax.sharding import PartitionSpec as P

SEG_LEN = 64
LEFT_SEGS = 8
REL_CLIP = 256


def passed_along(block, axis, distance):
    devices = range(lax.axis_size(axis))
    route = [(i - distance, i) for i in devices if i - distance in devices]
    return lax.ppermute(block, axis, route)


def band_matrix(diagonal_vals, row_count, col_count):
    head_count = diagonal_vals.shape[0]
    span_width = row_count + col_count - 1
    repeated = jnp.broadcast_to(diagonal_vals[:, None, :], (head_count, row_count, span_width))
    flat_rows = jnp.pad(
        repeated.reshape(head_count, row_count * span_width), ((0, 0), (0, row_count))
    )
    shaped = flat_rows.reshape(head_count, row_count, span_width + 1)[:, :, :col_count]
    return shaped[:, :, ::-1]


def diagonal_sums(matrix_vals):
    head_count, row_count, col_count = matrix_vals.shape
    span_width = row_count + col_count - 1
    flipped = jnp.pad(matrix_vals[:, :, ::-1], ((0, 0), (0, 0), (0, row_count)))
    skewed = flipped.reshape(head_count, row_count * (col_count + row_count))[
        :, : row_count * span_width
    ]
    return jnp.sum(skewed.reshape(head_count, row_count, span_width), axis=1)


def table_onehot(offset, row_count, col_count, table_len):
    diagonals = jnp.arange(row_count + col_count - 1, dtype=jnp.int32)
    distance = jnp.clip(offset + diagonals - (col_count - 1), 1 - SEG_LEN, REL_CLIP) + SEG_LEN - 1
    return (distance[:, None] == jnp.arange(table_len, dtype=jnp.int32)[None, :]).astype(
        jnp.float32
    )


def bias_block(bias_table, offset, row_count, col_count):
    onehot_map = table_onehot(offset, row_count, col_count, bias_table.shape[1])
    diagonal_vals = jnp.dot(bias_table, onehot_map.T, precision=lax.Precision.HIGHEST)
    return (band_matrix(diagonal_vals, row_count, col_count), onehot_map)


def band_stack(rows, block_count, span_segs):
    segmented = rows.reshape(-1, SEG_LEN, rows.shape[1])
    pieces = [segmented[start : start + block_count] for start in range(span_segs)]
    return jnp.stack(pieces, axis=1).reshape(block_count, span_segs * SEG_LEN, rows.shape[1])


def band_terms(queries, grads_out, log_rows, dot_rows, keys, values, bias_vals, allowed):
    block_count, query_count, feature_count = queries.shape
    key_count = keys.shape[1]
    head_count = log_rows.shape[2]
    query_heads = queries.reshape(block_count, query_count, head_count, -1)
    grad_heads = grads_out.reshape(block_count, query_count, head_count, -1)
    key_heads = keys.reshape(block_count, key_count, head_count, -1)
    value_heads = values.reshape(block_count, key_count, head_count, -1)
    inv_root = query_heads.shape[3] ** (-0.5)
    raw_scores = jnp.einsum(
        "bqhd,bkhd->bhqk", query_heads, key_heads, preferred_element_type=jnp.float32
    )
    scores = raw_scores * inv_root + bias_vals[None]
    log_terms = jnp.transpose(log_rows, (0, 2, 1))[:, :, :, None]
    dot_terms = jnp.transpose(dot_rows, (0, 2, 1))[:, :, :, None]
    weights = jnp.exp(scores - log_terms)
    weights = jnp.where(allowed[:, None, None, :], weights, 0.0)
    weight_grads = jnp.einsum(
        "bqhd,bkhd->bhqk", grad_heads, value_heads, preferred_element_type=jnp.float32
    )
    score_grads = weights * (weight_grads - dot_terms)
    return (
        weights.astype(jnp.bfloat16),
        score_grads.astype(jnp.bfloat16),
        score_grads,
        query_heads,
        key_heads,
        grad_heads,
        inv_root,
    )


def local(query_rows, key_rows, value_rows, out_grad, log_totals, out_dot, bias_table):
    row_count = query_rows.shape[0]
    feature_count = query_rows.shape[1]
    head_count = log_totals.shape[1]
    seg_count = row_count // SEG_LEN
    span_segs = LEFT_SEGS + 1
    band_len = span_segs * SEG_LEN
    need_rows = LEFT_SEGS * SEG_LEN
    lag_total = -(-need_rows // row_count)
    skip_rows = lag_total * row_count - need_rows
    first_row = lax.axis_index(("sp", "tp")) * row_count
    earlier = []
    for lag_count in range(lag_total, 0, -1):
        start_row = skip_rows if lag_count == lag_total else 0
        earlier.append(passed_along((key_rows, value_rows), ("sp", "tp"), lag_count))
    all_keys = jnp.concatenate([pair[0] for pair in earlier] + [key_rows], axis=0)
    all_values = jnp.concatenate([pair[1] for pair in earlier] + [value_rows], axis=0)
    key_bands = band_stack(all_keys, seg_count, span_segs)
    value_bands = band_stack(all_values, seg_count, span_segs)
    band_pos = (
        jnp.arange(seg_count, dtype=jnp.int32)[:, None] * SEG_LEN
        + jnp.arange(band_len, dtype=jnp.int32)[None, :]
    )
    allowed = first_row - need_rows + band_pos >= 0
    bias_vals, onehot_map = bias_block(bias_table, need_rows, SEG_LEN, band_len)
    weights_b, score_grads_b, score_grads, query_heads, key_heads, grad_heads, inv_root = (
        band_terms(
            query_rows.reshape(seg_count, SEG_LEN, feature_count),
            out_grad.reshape(seg_count, SEG_LEN, feature_count),
            log_totals.reshape(seg_count, SEG_LEN, head_count),
            out_dot.reshape(seg_count, SEG_LEN, head_count),
            key_bands,
            value_bands,
            bias_vals,
            allowed,
        )
    )
    tap_part = jnp.dot(
        diagonal_sums(jnp.sum(score_grads, axis=0)), onehot_map, precision=lax.Precision.HIGHEST
    )
    query_part = jnp.einsum(
        "bhqk,bkhd->bqhd", score_grads_b, key_heads, preferred_element_type=jnp.float32
    )
    grad_query = (query_part * inv_root).reshape(row_count, feature_count).astype(jnp.bfloat16)
    key_band_grad = jnp.einsum(
        "bhqk,bqhd->bkhd", score_grads_b, query_heads, preferred_element_type=jnp.float32
    )
    key_band_grad = (key_band_grad * inv_root).reshape(seg_count, span_segs, SEG_LEN, feature_count)
    value_band_grad = jnp.einsum(
        "bhqk,bqhd->bkhd", weights_b, grad_heads, preferred_element_type=jnp.float32
    )
    value_band_grad = value_band_grad.reshape(seg_count, span_segs, SEG_LEN, feature_count)
    key_all = sum(
        (
            jnp.pad(key_band_grad[:, lag], ((lag, LEFT_SEGS - lag), (0, 0), (0, 0)))
            for lag in range(span_segs)
        )
    ).reshape(-1, feature_count)
    value_all = sum(
        (
            jnp.pad(value_band_grad[:, lag], ((lag, LEFT_SEGS - lag), (0, 0), (0, 0)))
            for lag in range(span_segs)
        )
    ).reshape(-1, feature_count)
    key_total = key_all[need_rows:]
    value_total = value_all[need_rows:]
    for lag_count in range(1, lag_total + 1):
        lower_row = max(need_rows - lag_count * row_count, 0)
        upper_row = need_rows - (lag_count - 1) * row_count
        returned = passed_along(
            (key_all[lower_row:upper_row], value_all[lower_row:upper_row]), ("sp", "tp"), -lag_count
        )
        lead_rows = row_count - (upper_row - lower_row)
        key_total = key_total + returned[0]
        value_total = value_total + returned[1]
    grad_table = lax.psum(tap_part, ("sp", "tp"))
    return (
        grad_query,
        key_total.astype(jnp.bfloat16),
        value_total.astype(jnp.bfloat16),
        grad_table,
    )


def solution(mesh):
    placed = (
        P(("sp", "tp"), None),
        P(("sp", "tp"), None),
        P(("sp", "tp"), None),
        P(("sp", "tp"), None),
        P(("sp", "tp"), None),
        P(("sp", "tp"), None),
        P(),
    )
    return jax.shard_map(
        local,
        mesh=mesh,
        in_specs=placed,
        out_specs=(P(("sp", "tp"), None), P(("sp", "tp"), None), P(("sp", "tp"), None), P()),
        check_vma=False,
    )
```

profile of v0, /device:TPU:0, one launch (start us, length us, event | category | flops | bytes accessed | tf_op | source)
XLA Modules:
  0.0 198.3 jit_solution(5561602564015735739)
XLA Ops:
  0.6 5.7 %collective-permute-start.1 = (bf16[256,1024]{1,0:T(8,128)(2,1)}, bf16[256,1024]{1,0:T(8,128)(2,1)}, u32[]{:S(2)}, u32[]{:S(2)}) collective-permute-start(bf16[256,1024]{1,0:T(8,128)(2,1)} %param.8), channel_id=1, source_target_pairs={{0,1},{1,2},{2,3},{3,4},{4,5},{5,6},{6,7},{7,8},{8,9},{9,10},{10,1... | collective-permute-start | bytes 1572872 | tf_op jit(solution)/shard_map/ppermute | solution.py:14
  6.3 2.1 %collective-permute-start = (bf16[256,1024]{1,0:T(8,128)(2,1)}, bf16[256,1024]{1,0:T(8,128)(2,1)}, u32[]{:S(2)}, u32[]{:S(2)}) collective-permute-start(bf16[256,1024]{1,0:T(8,128)(2,1)} %param.8), channel_id=1, source_target_pairs={{0,2},{1,3},{2,4},{3,5},{4,6},{5,7},{6,8},{7,9},{8,10},{9,11},{10,... | collective-permute-start | bytes 1572872 | tf_op jit(solution)/shard_map/ppermute | solution.py:14
  8.4 4.1 %collective-permute-start.3 = (bf16[256,1024]{1,0:T(8,128)(2,1)}, bf16[256,1024]{1,0:T(8,128)(2,1)}, u32[]{:S(2)}, u32[]{:S(2)}) collective-permute-start(bf16[256,1024]{1,0:T(8,128)(2,1)} %param.9), channel_id=1, source_target_pairs={{0,1},{1,2},{2,3},{3,4},{4,5},{5,6},{6,7},{7,8},{8,9},{9,10},{10,1... | collective-permute-start | bytes 1572872 | tf_op jit(solution)/shard_map/ppermute | solution.py:14
  12.6 2.1 %collective-permute-start.2 = (bf16[256,1024]{1,0:T(8,128)(2,1)}, bf16[256,1024]{1,0:T(8,128)(2,1)}, u32[]{:S(2)}, u32[]{:S(2)}) collective-permute-start(bf16[256,1024]{1,0:T(8,128)(2,1)} %param.9), channel_id=1, source_target_pairs={{0,2},{1,3},{2,4},{3,5},{4,6},{5,7},{6,8},{7,9},{8,10},{9,11},{10,... | collective-permute-start | bytes 1572872 | tf_op jit(solution)/shard_map/ppermute | solution.py:14
  18.1 1.9 copy.175
  24.6 3.6 %collective-permute-done.3 = bf16[256,1024]{1,0:T(8,128)(2,1)} collective-permute-done((bf16[256,1024]{1,0:T(8,128)(2,1)}, bf16[256,1024]{1,0:T(8,128)(2,1)}, u32[]{:S(2)}, u32[]{:S(2)}) %collective-permute-start.3) | collective-permute-done | bytes 524320 | tf_op jit(solution)/shard_map/ppermute | solution.py:14
  39.1 1.7 fusion.5
  41.3 5.0 %convolution_bitcast_fusion = f32[4,576,8,128]{3,1,2,0:T(8,128)} fusion(f32[4,8,576,64]{2,3,1,0:T(8,128)S(1)} %fusion.5, f32[4,8,64]{2,1,0:T(8,128)S(1)} %get-tuple-element.49, f32[8,64,576]{2,1,0:T(8,128)S(1)} %slice.268, pred[4,576]{1,0:T(4,128)(4,1)S(1)} %add_compare_fusion, bf16[4,64,8,128]{3,2,1,0:T(8,128)(2,1)S(1)} %bitcast.221), kind=kOutput, calls=%fused_computation.13 | convolution fusion | flops 307888128 | bytes 15870208 | tf_op jit(solution)/shard_map/bhqk,bqhd->bkhd/dot_general | solution.py:138
  46.3 4.2 %fusion.52 = (f32[8,64,576]{2,1,0:T(8,128)S(1)}, bf16[4,8,64,576]{3,2,1,0:T(8,128)(2,1)}) fusion(f32[4,8,64]{2,1,0:T(8,128)S(1)} %get-tuple-element.48, bf16[4,64,8,128]{3,2,1,0:T(8,128)(2,1)S(1)} %bitcast.222, bf16[4,576,8,128]{3,2,1,0:T(8,128)(2,1)S(1)} %bitcast.220, f32[4,8,64]{2,1,0:T(8,128)S(1)} %get-tuple-element.49, f32[8,64,576]{2,1,0:T(8,128)S(1)} %slice.268, ...), kind=kOutput, calls=%fused_computation.101 | convolution fusion | flops 311132160 | bytes 14698752 | tf_op jit(solution)/shard_map/bqhd,bkhd->bhqk/dot_general | solution.py:75
  52.8 1.3 reshape.121
  54.2 12.8 %copy.146 = f32[4,576,8,128]{3,2,1,0:T(8,128)} copy(f32[4,576,8,128]{3,1,2,0:T(8,128)} %convolution_bitcast_fusion) | data formatting | bytes 18874368 | tf_op jit(solution)/shard_map/bhqk,bqhd->bkhd/transpose | solution.py:138
  67.0 11.2 %reshape.119 = f32[4,9,64,1024]{3,2,1,0:T(8,128)} reshape(f32[4,576,8,128]{3,2,1,0:T(8,128)} %copy.146) | data formatting | bytes 18874368 | tf_op jit(solution)/shard_map/reshape | solution.py:141
  78.2 4.7 %slice_bitcast_fusion.8 = (f32[4,64,1024]{2,1,0:T(8,128)S(1)}, f32[4,64,1024]{2,1,0:T(8,128)S(1)}, f32[4,64,1024]{2,1,0:T(8,128)S(1)}, f32[4,64,1024]{2,1,0:T(8,...) fusion(f32[4,9,64,1024]{3,2,1,0:T(8,128)} %reshape.119), kind=kLoop, calls=%fused_computation.37 | loop fusion | bytes 18874368 | tf_op jit(solution)/shard_map/squeeze | solution.py:150
  83.8 1.6 fusion.46
  86.8 1.5 collective-permute-start.6
  88.3 1.5 multiply_bitcast_fusion
  89.8 9.1 %copy.136 = f32[4,576,8,128]{3,2,1,0:T(8,128)} copy(f32[4,576,8,128]{3,1,2,0:T(8,128)S(1)} %multiply_bitcast_fusion) | data formatting | bytes 18874368 | tf_op jit(solution)/shard_map/mul | solution.py:137
  98.9 11.1 %reshape.118 = f32[4,9,64,1024]{3,2,1,0:T(8,128)} reshape(f32[4,576,8,128]{3,2,1,0:T(8,128)} %copy.136) | data formatting | bytes 18874368 | tf_op jit(solution)/shard_map/reshape | solution.py:137
  110.0 4.7 %slice_bitcast_fusion.17 = (f32[4,64,1024]{2,1,0:T(8,128)S(1)}, f32[4,64,1024]{2,1,0:T(8,128)S(1)}, f32[4,64,1024]{2,1,0:T(8,128)S(1)}, f32[4,64,1024]{2,1,0:T(8...) fusion(f32[4,9,64,1024]{3,2,1,0:T(8,128)} %reshape.118), kind=kLoop, calls=%fused_computation.46 | loop fusion | bytes 18874368 | tf_op jit(solution)/shard_map/squeeze | solution.py:144
  115.8 1.7 fusion.47
  117.5 1.4 collective-permute-start.5
  123.2 70.2 %psum.7 = f32[8,320]{1,0:T(8,128)} all-reduce(f32[8,320]{1,0:T(8,128)S(1)} %fusion.37), channel_id=1, replica_groups=mesh['sp'=16,'tp'=2] {'sp','tp'}, use_global_device_ids=true, to_apply=%region_2.3 | all-reduce | flops 2560 | bytes 20480 | tf_op jit(solution)/shard_map/psum | solution.py:165
  193.4 2.6 %fusion.34 = bf16[256,1024]{1,0:T(8,128)(2,1)} fusion(f32[256,1024]{1,0:T(8,128)} %collective-permute-done.7, f32[256,1024]{1,0:T(8,128)} %collective-permute-done.6, f32[4,64,1024]{2,1,0:T(8,128)S(1)} %get-tuple-element.22), kind=kLoop, calls=%fused_computation.49 | loop fusion | flops 786432 | bytes 3670016 | tf_op jit(solution)/shard_map/convert_element_type | solution.py:169
  196.0 2.3 %fusion.36 = bf16[256,1024]{1,0:T(8,128)(2,1)} fusion(f32[256,1024]{1,0:T(8,128)S(1)} %collective-permute-done.5, f32[256,1024]{1,0:T(8,128)} %collective-permute-done.4, f32[4,64,1024]{2,1,0:T(8,128)S(1)} %get-tuple-element.25), kind=kLoop, calls=%fused_computation.52 | loop fusion | flops 786432 | bytes 3670016 | tf_op jit(solution)/shard_map/convert_element_type | solution.py:168
  (83 shorter events, 28.8 us)
Async XLA Ops:
  0.6 14.0 %copy-start = (f32[8,320]{1,0:T(8,128)S(1)}, f32[8,320]{1,0:T(8,128)}, u32[]{:S(2)}) copy-start(f32[8,320]{1,0:T(8,128)} %param.13) | copy-start | bytes 30724
  0.6 29.3 %collective-permute-start.1 = (bf16[256,1024]{1,0:T(8,128)(2,1)}, bf16[256,1024]{1,0:T(8,128)(2,1)}, u32[]{:S(2)}, u32[]{:S(2)}) collective-permute-start(bf16[256,1024]{1,0:T(8,128)(2,1)} %param.8), channel_id=1, source_target_pairs={{0,1},{1,2},{2,3},{3,4},{4,5},{5,6},{6,7},{7,8},{8,9},{9,10},{10,1... | collective-permute-start | bytes 1572872 | tf_op jit(solution)/shard_map/ppermute | solution.py:14
  6.3 17.2 %collective-permute-start = (bf16[256,1024]{1,0:T(8,128)(2,1)}, bf16[256,1024]{1,0:T(8,128)(2,1)}, u32[]{:S(2)}, u32[]{:S(2)}) collective-permute-start(bf16[256,1024]{1,0:T(8,128)(2,1)} %param.8), channel_id=1, source_target_pairs={{0,2},{1,3},{2,4},{3,5},{4,6},{5,7},{6,8},{7,9},{8,10},{9,11},{10,... | collective-permute-start | bytes 1572872 | tf_op jit(solution)/shard_map/ppermute | solution.py:14
  8.4 19.8 %collective-permute-start.3 = (bf16[256,1024]{1,0:T(8,128)(2,1)}, bf16[256,1024]{1,0:T(8,128)(2,1)}, u32[]{:S(2)}, u32[]{:S(2)}) collective-permute-start(bf16[256,1024]{1,0:T(8,128)(2,1)} %param.9), channel_id=1, source_target_pairs={{0,1},{1,2},{2,3},{3,4},{4,5},{5,6},{6,7},{7,8},{8,9},{9,10},{10,1... | collective-permute-start | bytes 1572872 | tf_op jit(solution)/shard_map/ppermute | solution.py:14
  12.6 9.9 %collective-permute-start.2 = (bf16[256,1024]{1,0:T(8,128)(2,1)}, bf16[256,1024]{1,0:T(8,128)(2,1)}, u32[]{:S(2)}, u32[]{:S(2)}) collective-permute-start(bf16[256,1024]{1,0:T(8,128)(2,1)} %param.9), channel_id=1, source_target_pairs={{0,2},{1,3},{2,4},{3,5},{4,6},{5,7},{6,8},{7,9},{8,10},{9,11},{10,... | collective-permute-start | bytes 1572872 | tf_op jit(solution)/shard_map/ppermute | solution.py:14
  22.0 7.4 %copy-start.6 = (bf16[256,1024]{1,0:T(8,128)(2,1)S(1)}, bf16[256,1024]{1,0:T(8,128)(2,1)}, u32[]{:S(2)}) copy-start(bf16[256,1024]{1,0:T(8,128)(2,1)} %param.9) | copy-start | bytes 1572868
  29.4 1.7 copy-start.7
  39.0 2.2 %copy-start.2 = (bf16[288,8,8,128]{3,2,1,0:T(8,128)(2,1)}, bf16[288,8,8,128]{3,2,1,0:T(8,128)(2,1)S(1)}, u32[]{:S(2)}) copy-start(bf16[288,8,8,128]{3,2,1,0:T(8,128)(2,1)S(1)} %copy.171) | copy-start | bytes 14155780
  39.1 2.2 %copy-start.5 = (bf16[32,8,8,128]{3,2,1,0:T(8,128)(2,1)S(1)}, bf16[32,8,8,128]{3,2,1,0:T(8,128)(2,1)}, u32[]{:S(2)}) copy-start(bf16[32,8,8,128]{3,2,1,0:T(8,128)(2,1)} %copy.175) | copy-start | bytes 1572868
  83.8 4.5 %copy-start.3 = (bf16[4,8,64,576]{3,2,1,0:T(8,128)(2,1)S(1)}, bf16[4,8,64,576]{3,2,1,0:T(8,128)(2,1)}, u32[]{:S(2)}) copy-start(bf16[4,8,64,576]{3,2,1,0:T(8,128)(2,1)} %get-tuple-element.45) | copy-start | bytes 7077892
  85.5 107.9 %collective-permute-start.7 = (f32[256,1024]{1,0:T(8,128)}, f32[256,1024]{1,0:T(8,128)}, u32[]{:S(2)}, u32[]{:S(2)}) collective-permute-start(f32[256,1024]{1,0:T(8,128)} %bitcast.67), channel_id=1, source_target_pairs={{2,0},{3,1},{4,2},{5,3},{6,4},{7,5},{8,6},{9,7},{10,8},{11,9},{12,... | collective-permute-start | bytes 3145736 | tf_op jit(solution)/shard_map/ppermute | solution.py:14
  86.8 106.6 %collective-permute-start.6 = (f32[256,1024]{1,0:T(8,128)}, f32[256,1024]{1,0:T(8,128)}, u32[]{:S(2)}, u32[]{:S(2)}) collective-permute-start(f32[256,1024]{1,0:T(8,128)} %bitcast.66), channel_id=1, source_target_pairs={{1,0},{2,1},{3,2},{4,3},{5,4},{6,5},{7,6},{8,7},{9,8},{10,9},{11,1... | collective-permute-start | bytes 3145736 | tf_op jit(solution)/shard_map/ppermute | solution.py:14
  110.0 10.2 %slice-start = ((s8[4718592]{0:T(1024)(128)(4,1)}), s8[524288]{0:T(1024)(128)(4,1)S(1)}, s32[]{:S(2)}) async-start(s8[4718592]{0:T(1024)(128)(4,1)} %bitcast.210), calls=%async_computation | async-start | bytes 1048576
  114.8 5.4 %slice-start.1 = ((s8[4718592]{0:T(1024)(128)(4,1)}), s8[4194304]{0:T(1024)(128)(4,1)S(1)}, s32[]{:S(2)}) async-start(s8[4718592]{0:T(1024)(128)(4,1)} %bitcast.210), calls=%async_computation.1 | async-start | bytes 8388608
  115.8 4.4 %copy-start.4 = (bf16[4,8,64,576]{3,2,1,0:T(8,128)(2,1)S(1)}, bf16[4,8,64,576]{3,2,1,0:T(8,128)(2,1)}, u32[]{:S(2)}) copy-start(bf16[4,8,64,576]{3,2,1,0:T(8,128)(2,1)} %get-tuple-element.45) | copy-start | bytes 7077892
  117.5 78.5 %collective-permute-start.5 = (f32[256,1024]{1,0:T(8,128)}, f32[256,1024]{1,0:T(8,128)S(1)}, u32[]{:S(2)}, u32[]{:S(2)}) collective-permute-start(f32[256,1024]{1,0:T(8,128)} %bitcast.54), channel_id=1, source_target_pairs={{2,0},{3,1},{4,2},{5,3},{6,4},{7,5},{8,6},{9,7},{10,8},{11,9},{12,... | collective-permute-start | bytes 3145736 | tf_op jit(solution)/shard_map/ppermute | solution.py:14
  118.9 77.1 %collective-permute-start.4 = (f32[256,1024]{1,0:T(8,128)}, f32[256,1024]{1,0:T(8,128)}, u32[]{:S(2)}, u32[]{:S(2)}) collective-permute-start(f32[256,1024]{1,0:T(8,128)} %bitcast.53), channel_id=1, source_target_pairs={{1,0},{2,1},{3,2},{4,3},{5,4},{6,5},{7,6},{8,7},{9,8},{10,9},{11,1... | collective-permute-start | bytes 3145736 | tf_op jit(solution)/shard_map/ppermute | solution.py:14
  120.2 78.0 %copy-start.1 = (f32[8,320]{1,0:T(8,128)S(1)}, f32[8,320]{1,0:T(8,128)}, u32[]{:S(2)}) copy-start(f32[8,320]{1,0:T(8,128)} %param.13) | copy-start | bytes 30724
where the time goes:
time: 200 us; the launch traced here: 198 us
  local copies, waits for them, and re-layouts  81.9 us (41%)
  blocking collectives  70.2 us (35%)
  starting transfers between devices  19.5 us (10%)
  matrix products  14.8 us (7%)
  other arithmetic  7.04 us (4%)
  waiting for transfers between devices  3.66 us (2%)
    psum x1, blocking collectives, local(): grad_table = lax.psum(tap_part, ('sp', 'tp'))  70.2 us
    unnamed x52, local copies, waits for them, and re-layouts  19.8 us
    ppermute x8, starting transfers between devices, passed_along(): return lax.ppermute(block, axis, route)  19.5 us
    transpose x1, local copies, waits for them, and re-layouts, local(): jnp.einsum('bhqk,bqhd->bkhd', weights_b, grad_heads, preferred_element_ty...  12.8 us
    reshape x1, local copies, waits for them, and re-layouts, local(): value_band_grad.reshape(seg_count, span_segs, SEG_LEN, feature_count)  11.2 us
    reshape x1, local copies, waits for them, and re-layouts, local(): (key_band_grad * inv_root).reshape(seg_count, span_segs, SEG_LEN, feature...  11.1 us
    mul x1, local copies, waits for them, and re-layouts, local(): key_band_grad * inv_root  9.13 us
    dot_general x1, matrix products, local(): jnp.einsum('bhqk,bqhd->bkhd', weights_b, grad_heads, preferred_element_ty...  5.01 us
  transfers between devices with their start and end apart: 8, of which 1 were waited for; matrix products, arithmetic and copies ran while one was open for 23% of the time, Pallas kernels for 0%

commit v1 on v0

--- a/solution.py
+++ b/solution.py
@@ -1,11 +1,22 @@
+import functools
 import jax
 import jax.numpy as jnp
 from jax import lax
 from jax.sharding import PartitionSpec as P
+from jax.lax import psum
 
 SEG_LEN = 64
 LEFT_SEGS = 8
 REL_CLIP = 256
+
+
+def refer_bench(base_x, mesh_name, mesh_ax):
+    for idx in (mesh_name, mesh_ax):
+        base_x = psum(base_x, idx)
+    return base_x
+
+
+page_plan = functools.partial(refer_bench, mesh_name="tp", mesh_ax="sp")
 
 
 def passed_along(block, axis, distance):
@@ -162,7 +173,7 @@
         lead_rows = row_count - (upper_row - lower_row)
         key_total = key_total + returned[0]
         value_total = value_total + returned[1]
-    grad_table = lax.psum(tap_part, ("sp", "tp"))
+    grad_table = page_plan(tap_part)
     return (
         grad_query,
         key_total.astype(jnp.bfloat16),

time: 200 us -> 228 us (1.14)
  blocking collectives: 70.2 us -> 98.6 us
    psum x1 -> x2, blocking collectives: 70.2 us -> 98.6 us  [refer_bench(): base_x = psum(base_x, idx)]
  transfers between devices with their start and end apart: 8 -> 8, of which waited for: 1 -> 1; matrix products, arithmetic and copies ran while one was open for 23% -> 20% of each run, Pallas kernels for 0% -> 0%
where the time goes in v1:
time: 228 us; the launch traced here: 227 us
  blocking collectives  98.6 us (43%)
  local copies, waits for them, and re-layouts  82 us (36%)
  starting transfers between devices  19.5 us (9%)
  matrix products  14.8 us (6%)
  other arithmetic  7.03 us (3%)
  waiting for transfers between devices  3.63 us (2%)
    psum x2, blocking collectives, refer_bench(): base_x = psum(base_x, idx)  98.6 us
    unnamed x52, local copies, waits for them, and re-layouts  19.8 us
    ppermute x8, starting transfers between devices, passed_along(): return lax.ppermute(block, axis, route)  19.5 us
    transpose x1, local copies, waits for them, and re-layouts, local(): jnp.einsum('bhqk,bqhd->bkhd', weights_b, grad_heads, preferred_element_ty...  12.8 us
    reshape x1, local copies, waits for them, and re-layouts, local(): value_band_grad.reshape(seg_count, span_segs, SEG_LEN, feature_count)  11.2 us
    reshape x1, local copies, waits for them, and re-layouts, local(): (key_band_grad * inv_root).reshape(seg_count, span_segs, SEG_LEN, feature...  11.1 us
    mul x1, local copies, waits for them, and re-layouts, local(): key_band_grad * inv_root  9.11 us
    dot_general x1, matrix products, local(): jnp.einsum('bhqk,bqhd->bkhd', weights_b, grad_heads, preferred_element_ty...  4.99 us
  transfers between devices with their start and end apart: 8, of which 1 were waited for; matrix products, arithmetic and copies ran while one was open for 20% of the time, Pallas kernels for 0%

profile of v1, /device:TPU:0, one launch (start us, length us, event | category | flops | bytes accessed | tf_op | source)
XLA Modules:
  0.0 226.7 jit_solution(13026739323105482837)
XLA Ops:
  0.6 5.7 %collective-permute-start.1 = (bf16[256,1024]{1,0:T(8,128)(2,1)}, bf16[256,1024]{1,0:T(8,128)(2,1)}, u32[]{:S(2)}, u32[]{:S(2)}) collective-permute-start(bf16[256,1024]{1,0:T(8,128)(2,1)} %param.8), channel_id=1, source_target_pairs={{0,1},{1,2},{2,3},{3,4},{4,5},{5,6},{6,7},{7,8},{8,9},{9,10},{10,1... | collective-permute-start | bytes 1572872 | tf_op jit(solution)/shard_map/ppermute | solution.py:25
  6.3 2.1 collective-permute-start
  8.4 4.2 %collective-permute-start.3 = (bf16[256,1024]{1,0:T(8,128)(2,1)}, bf16[256,1024]{1,0:T(8,128)(2,1)}, u32[]{:S(2)}, u32[]{:S(2)}) collective-permute-start(bf16[256,1024]{1,0:T(8,128)(2,1)} %param.9), channel_id=1, source_target_pairs={{0,1},{1,2},{2,3},{3,4},{4,5},{5,6},{6,7},{7,8},{8,9},{9,10},{10,1... | collective-permute-start | bytes 1572872 | tf_op jit(solution)/shard_map/ppermute | solution.py:25
  12.6 2.1 collective-permute-start.2
  18.1 1.9 copy.175
  24.6 3.6 %collective-permute-done.3 = bf16[256,1024]{1,0:T(8,128)(2,1)} collective-permute-done((bf16[256,1024]{1,0:T(8,128)(2,1)}, bf16[256,1024]{1,0:T(8,128)(2,1)}, u32[]{:S(2)}, u32[]{:S(2)}) %collective-permute-start.3) | collective-permute-done | bytes 524320 | tf_op jit(solution)/shard_map/ppermute | solution.py:25
  39.1 1.7 fusion.5
  41.3 5.0 %convolution_bitcast_fusion = f32[4,576,8,128]{3,1,2,0:T(8,128)} fusion(f32[4,8,576,64]{2,3,1,0:T(8,128)S(1)} %fusion.5, f32[4,8,64]{2,1,0:T(8,128)S(1)} %get-tuple-element.49, f32[8,64,576]{2,1,0:T(8,128)S(1)} %slice.268, pred[4,576]{1,0:T(4,128)(4,1)S(1)} %add_compare_fusion, bf16[4,64,8,128]{3,2,1,0:T(8,128)(2,1)S(1)} %bitcast.221), kind=kOutput, calls=%fused_computation.13 | convolution fusion | flops 307888128 | bytes 15870208 | tf_op jit(solution)/shard_map/bhqk,bqhd->bkhd/dot_general | solution.py:149
  46.2 4.3 %fusion.52 = (f32[8,64,576]{2,1,0:T(8,128)S(1)}, bf16[4,8,64,576]{3,2,1,0:T(8,128)(2,1)}) fusion(f32[4,8,64]{2,1,0:T(8,128)S(1)} %get-tuple-element.48, bf16[4,64,8,128]{3,2,1,0:T(8,128)(2,1)S(1)} %bitcast.222, bf16[4,576,8,128]{3,2,1,0:T(8,128)(2,1)S(1)} %bitcast.220, f32[4,8,64]{2,1,0:T(8,128)S(1)} %get-tuple-element.49, f32[8,64,576]{2,1,0:T(8,128)S(1)} %slice.268, ...), kind=kOutput, calls=%fused_computation.101 | convolution fusion | flops 311132160 | bytes 14698752 | tf_op jit(solution)/shard_map/bqhd,bkhd->bhqk/dot_general | solution.py:86
  54.2 12.8 %copy.146 = f32[4,576,8,128]{3,2,1,0:T(8,128)} copy(f32[4,576,8,128]{3,1,2,0:T(8,128)} %convolution_bitcast_fusion) | data formatting | bytes 18874368 | tf_op jit(solution)/shard_map/bhqk,bqhd->bkhd/transpose | solution.py:149
  67.0 11.2 %reshape.119 = f32[4,9,64,1024]{3,2,1,0:T(8,128)} reshape(f32[4,576,8,128]{3,2,1,0:T(8,128)} %copy.146) | data formatting | bytes 18874368 | tf_op jit(solution)/shard_map/reshape | solution.py:152
  78.2 4.7 %slice_bitcast_fusion.8 = (f32[4,64,1024]{2,1,0:T(8,128)S(1)}, f32[4,64,1024]{2,1,0:T(8,128)S(1)}, f32[4,64,1024]{2,1,0:T(8,128)S(1)}, f32[4,64,1024]{2,1,0:T(8,...) fusion(f32[4,9,64,1024]{3,2,1,0:T(8,128)} %reshape.119), kind=kLoop, calls=%fused_computation.37 | loop fusion | bytes 18874368 | tf_op jit(solution)/shard_map/squeeze | solution.py:161
  83.9 1.6 fusion.46
  86.8 1.5 collective-permute-start.6
  88.3 1.5 multiply_bitcast_fusion
  89.8 9.1 %copy.136 = f32[4,576,8,128]{3,2,1,0:T(8,128)} copy(f32[4,576,8,128]{3,1,2,0:T(8,128)S(1)} %multiply_bitcast_fusion) | data formatting | bytes 18874368 | tf_op jit(solution)/shard_map/mul | solution.py:148
  98.9 11.1 %reshape.118 = f32[4,9,64,1024]{3,2,1,0:T(8,128)} reshape(f32[4,576,8,128]{3,2,1,0:T(8,128)} %copy.136) | data formatting | bytes 18874368 | tf_op jit(solution)/shard_map/reshape | solution.py:148
  110.0 4.7 %slice_bitcast_fusion.17 = (f32[4,64,1024]{2,1,0:T(8,128)S(1)}, f32[4,64,1024]{2,1,0:T(8,128)S(1)}, f32[4,64,1024]{2,1,0:T(8,128)S(1)}, f32[4,64,1024]{2,1,0:T(8...) fusion(f32[4,9,64,1024]{3,2,1,0:T(8,128)} %reshape.118), kind=kLoop, calls=%fused_computation.46 | loop fusion | bytes 18874368 | tf_op jit(solution)/shard_map/squeeze | solution.py:155
  115.8 1.7 fusion.47
  117.5 1.4 collective-permute-start.5
  123.2 21.6 %psum.14 = f32[8,320]{1,0:T(8,128)S(1)} all-reduce(f32[8,320]{1,0:T(8,128)S(1)} %fusion.37), channel_id=1, replica_groups=mesh['sp'=16,'tp'=2] {'tp'}, use_global_device_ids=true, to_apply=%region_2.3 | all-reduce | flops 2560 | bytes 20480 | tf_op jit(solution)/shard_map/psum | solution.py:15
  144.8 77.0 %psum.15 = f32[8,320]{1,0:T(8,128)} all-reduce(f32[8,320]{1,0:T(8,128)S(1)} %psum.14), channel_id=1, replica_groups=mesh['sp'=16,'tp'=2] {'sp'}, use_global_device_ids=true, to_apply=%region_3.4 | all-reduce | flops 2560 | bytes 20480 | tf_op jit(solution)/shard_map/psum | solution.py:15
  221.8 2.6 %fusion.34 = bf16[256,1024]{1,0:T(8,128)(2,1)} fusion(f32[256,1024]{1,0:T(8,128)} %collective-permute-done.7, f32[256,1024]{1,0:T(8,128)} %collective-permute-done.6, f32[4,64,1024]{2,1,0:T(8,128)S(1)} %get-tuple-element.22), kind=kLoop, calls=%fused_computation.49 | loop fusion | flops 786432 | bytes 3670016 | tf_op jit(solution)/shard_map/convert_element_type | solution.py:180
  224.4 2.3 %fusion.36 = bf16[256,1024]{1,0:T(8,128)(2,1)} fusion(f32[256,1024]{1,0:T(8,128)S(1)} %collective-permute-done.5, f32[256,1024]{1,0:T(8,128)} %collective-permute-done.4, f32[4,64,1024]{2,1,0:T(8,128)S(1)} %get-tuple-element.25), kind=kLoop, calls=%fused_computation.52 | loop fusion | flops 786432 | bytes 3670016 | tf_op jit(solution)/shard_map/convert_element_type | solution.py:179
  (84 shorter events, 30.1 us)
Async XLA Ops:
  0.6 14.1 %copy-start = (f32[8,320]{1,0:T(8,128)S(1)}, f32[8,320]{1,0:T(8,128)}, u32[]{:S(2)}) copy-start(f32[8,320]{1,0:T(8,128)} %param.13) | copy-start | bytes 30724
  0.6 29.3 %collective-permute-start.1 = (bf16[256,1024]{1,0:T(8,128)(2,1)}, bf16[256,1024]{1,0:T(8,128)(2,1)}, u32[]{:S(2)}, u32[]{:S(2)}) collective-permute-start(bf16[256,1024]{1,0:T(8,128)(2,1)} %param.8), channel_id=1, source_target_pairs={{0,1},{1,2},{2,3},{3,4},{4,5},{5,6},{6,7},{7,8},{8,9},{9,10},{10,1... | collective-permute-start | bytes 1572872 | tf_op jit(solution)/shard_map/ppermute | solution.py:25
  6.3 17.2 %collective-permute-start = (bf16[256,1024]{1,0:T(8,128)(2,1)}, bf16[256,1024]{1,0:T(8,128)(2,1)}, u32[]{:S(2)}, u32[]{:S(2)}) collective-permute-start(bf16[256,1024]{1,0:T(8,128)(2,1)} %param.8), channel_id=1, source_target_pairs={{0,2},{1,3},{2,4},{3,5},{4,6},{5,7},{6,8},{7,9},{8,10},{9,11},{10,... | collective-permute-start | bytes 1572872 | tf_op jit(solution)/shard_map/ppermute | solution.py:25
  8.4 19.8 %collective-permute-start.3 = (bf16[256,1024]{1,0:T(8,128)(2,1)}, bf16[256,1024]{1,0:T(8,128)(2,1)}, u32[]{:S(2)}, u32[]{:S(2)}) collective-permute-start(bf16[256,1024]{1,0:T(8,128)(2,1)} %param.9), channel_id=1, source_target_pairs={{0,1},{1,2},{2,3},{3,4},{4,5},{5,6},{6,7},{7,8},{8,9},{9,10},{10,1... | collective-permute-start | bytes 1572872 | tf_op jit(solution)/shard_map/ppermute | solution.py:25
  12.6 9.9 %collective-permute-start.2 = (bf16[256,1024]{1,0:T(8,128)(2,1)}, bf16[256,1024]{1,0:T(8,128)(2,1)}, u32[]{:S(2)}, u32[]{:S(2)}) collective-permute-start(bf16[256,1024]{1,0:T(8,128)(2,1)} %param.9), channel_id=1, source_target_pairs={{0,2},{1,3},{2,4},{3,5},{4,6},{5,7},{6,8},{7,9},{8,10},{9,11},{10,... | collective-permute-start | bytes 1572872 | tf_op jit(solution)/shard_map/ppermute | solution.py:25
  22.0 7.4 %copy-start.6 = (bf16[256,1024]{1,0:T(8,128)(2,1)S(1)}, bf16[256,1024]{1,0:T(8,128)(2,1)}, u32[]{:S(2)}) copy-start(bf16[256,1024]{1,0:T(8,128)(2,1)} %param.9) | copy-start | bytes 1572868
  29.4 1.7 copy-start.7
  39.0 2.2 copy-start.2
  39.1 2.2 copy-start.5
  83.9 4.5 %copy-start.3 = (bf16[4,8,64,576]{3,2,1,0:T(8,128)(2,1)S(1)}, bf16[4,8,64,576]{3,2,1,0:T(8,128)(2,1)}, u32[]{:S(2)}) copy-start(bf16[4,8,64,576]{3,2,1,0:T(8,128)(2,1)} %get-tuple-element.45) | copy-start | bytes 7077892
  85.5 136.3 %collective-permute-start.7 = (f32[256,1024]{1,0:T(8,128)}, f32[256,1024]{1,0:T(8,128)}, u32[]{:S(2)}, u32[]{:S(2)}) collective-permute-start(f32[256,1024]{1,0:T(8,128)} %bitcast.67), channel_id=1, source_target_pairs={{2,0},{3,1},{4,2},{5,3},{6,4},{7,5},{8,6},{9,7},{10,8},{11,9},{12,... | collective-permute-start | bytes 3145736 | tf_op jit(solution)/shard_map/ppermute | solution.py:25
  86.8 135.0 %collective-permute-start.6 = (f32[256,1024]{1,0:T(8,128)}, f32[256,1024]{1,0:T(8,128)}, u32[]{:S(2)}, u32[]{:S(2)}) collective-permute-start(f32[256,1024]{1,0:T(8,128)} %bitcast.66), channel_id=1, source_target_pairs={{1,0},{2,1},{3,2},{4,3},{5,4},{6,5},{7,6},{8,7},{9,8},{10,9},{11,1... | collective-permute-start | bytes 3145736 | tf_op jit(solution)/shard_map/ppermute | solution.py:25
  110.0 10.2 %slice-start = ((s8[4718592]{0:T(1024)(128)(4,1)}), s8[524288]{0:T(1024)(128)(4,1)S(1)}, s32[]{:S(2)}) async-start(s8[4718592]{0:T(1024)(128)(4,1)} %bitcast.210), calls=%async_computation | async-start | bytes 1048576
  114.8 5.4 %slice-start.1 = ((s8[4718592]{0:T(1024)(128)(4,1)}), s8[4194304]{0:T(1024)(128)(4,1)S(1)}, s32[]{:S(2)}) async-start(s8[4718592]{0:T(1024)(128)(4,1)} %bitcast.210), calls=%async_computation.1 | async-start | bytes 8388608
  115.8 4.4 %copy-start.4 = (bf16[4,8,64,576]{3,2,1,0:T(8,128)(2,1)S(1)}, bf16[4,8,64,576]{3,2,1,0:T(8,128)(2,1)}, u32[]{:S(2)}) copy-start(bf16[4,8,64,576]{3,2,1,0:T(8,128)(2,1)} %get-tuple-element.45) | copy-start | bytes 7077892
  117.5 106.9 %collective-permute-start.5 = (f32[256,1024]{1,0:T(8,128)}, f32[256,1024]{1,0:T(8,128)S(1)}, u32[]{:S(2)}, u32[]{:S(2)}) collective-permute-start(f32[256,1024]{1,0:T(8,128)} %bitcast.54), channel_id=1, source_target_pairs={{2,0},{3,1},{4,2},{5,3},{6,4},{7,5},{8,6},{9,7},{10,8},{11,9},{12,... | collective-permute-start | bytes 3145736 | tf_op jit(solution)/shard_map/ppermute | solution.py:25
  118.9 105.5 %collective-permute-start.4 = (f32[256,1024]{1,0:T(8,128)}, f32[256,1024]{1,0:T(8,128)}, u32[]{:S(2)}, u32[]{:S(2)}) collective-permute-start(f32[256,1024]{1,0:T(8,128)} %bitcast.53), channel_id=1, source_target_pairs={{1,0},{2,1},{3,2},{4,3},{5,4},{6,5},{7,6},{8,7},{9,8},{10,9},{11,1... | collective-permute-start | bytes 3145736 | tf_op jit(solution)/shard_map/ppermute | solution.py:25
  120.2 106.5 %copy-start.1 = (f32[8,320]{1,0:T(8,128)S(1)}, f32[8,320]{1,0:T(8,128)}, u32[]{:S(2)}) copy-start(f32[8,320]{1,0:T(8,128)} %param.13) | copy-start | bytes 30724
